TPU v7x, 32 devices: a whole 2x2x4 slice. The times are simulated.
32 devices in a mesh: ep: 4 (over y, x), tp: 8 (over z, core).
Axes of the slice: x: 2, y: 2, z: 4, core: 2. Of those that a mesh axis runs over, the one named last changes fastest.
Arguments:
- queries: bfloat16 [2048, 16, 128], P('ep', 'tp'), may hold values from -125 to 125
- keys: bfloat16 [2048, 16, 128], P('ep', 'tp'), may hold values from -9 to 9
- values: bfloat16 [2048, 16, 128], P('ep', 'tp'), may hold values from -6 to 6
- mixing: float32 [16], P('tp'), may hold values from 0.3 to 0.8
- head_gain: float32 [128], replicated, may hold values from 0.1 to 1.9
- out_weight: bfloat16 [16, 128, 2048], P('tp'), may hold values from -0.125 to 0.125
- tokens_b: bfloat16 [4096, 2048], P(('ep', 'tp')), may hold values from -6 to 6
- norm_gain: float32 [2048], replicated, may hold values from 0.1 to 1.9
- expert_ids: int32 [4096, 2], P(('ep', 'tp')), may hold values from 0 to 3, all different within a row; in each aligned block of 128 rows (0 to 127, 128 to 255, ...) at most 96 rows name the same one
- group_gate: float32 [4096], P(('ep', 'tp')), may hold values from 0.2 to 1
- expert_gate: float32 [4096, 2], P(('ep', 'tp')), may hold values from 0.1 to 0.9
- gate_weight: bfloat16 [4, 2048, 1024], P('ep', None, 'tp'), may hold values from -0.125 to 0.125
- up_weight: bfloat16 [4, 2048, 1024], P('ep', None, 'tp'), may hold values from -0.125 to 0.125
- down_weight: bfloat16 [4, 2048, 1024], P('ep', None, 'tp'), may hold values from -0.1875 to 0.1875
Outputs:
- mixed: bfloat16 [2048, 2048], P(('ep', 'tp'))
- routed: bfloat16 [4096, 2048], P(('ep', 'tp'))
Inputs may be any that keep to these rules, and one draw needn't show every extreme that they name: `expert_ids`: within each aligned block of 128 rows, no expert is named by more than 96 rows, and some block has an expert named by exactly 96 rows.
All inputs are finite; a program needn't handle non-finite values.
Results may differ from a plain program's by a relative error of at most 0.019.
Values may be sent and summed in bfloat16 or wider, within the bound.
A program may use at most 192 MiB of HBM per device.

v0:
```python
import math

import jax
import jax.numpy as jnp
from jax import lax
from jax.sharding import PartitionSpec as P

HEAD = 64


def attend_heads(queries, keys, values, mixing, head_gain):
    shard_rows = queries.shape[0]
    head_count = queries.shape[1]
    value_width = values.shape[2]
    query_start = lax.axis_index("ep") * shard_rows
    score_scale = 1.0 / math.sqrt(HEAD)
    query_pos = query_start + lax.iota(jnp.int32, shard_rows)

    def update(running, key_block, value_block, block_start):
        key_pos = block_start + lax.iota(jnp.int32, shard_rows)
        allowed = key_pos[None, :] <= query_pos[:, None]
        fresh = []
        for map_index in range(2):
            maximum, row_sum, numerator = running[3 * map_index : 3 * map_index + 3]
            offset = map_index * HEAD
            scores = (
                jnp.einsum(
                    "qhd,khd->hqk",
                    queries[:, :, offset : offset + HEAD],
                    key_block[:, :, offset : offset + HEAD],
                    preferred_element_type=jnp.float32,
                )
                * score_scale
            )
            scores = jnp.where(allowed[None], scores, -1e30)
            newmax = jnp.maximum(maximum, jnp.max(scores, axis=2))
            shrink = jnp.exp(maximum - newmax)
            weights = jnp.exp(scores - newmax[:, :, None])
            row_sum = row_sum * shrink + jnp.sum(weights, axis=2)
            numerator = numerator * shrink[:, :, None] + jnp.einsum(
                "hqk,khe->hqe",
                weights.astype(jnp.bfloat16),
                value_block,
                preferred_element_type=jnp.float32,
            )
            fresh += [newmax, row_sum, numerator]
        return tuple(fresh)

    floor_max = jnp.full((head_count, shard_rows), -1e30, jnp.float32)
    zero_sum = jnp.zeros((head_count, shard_rows), jnp.float32)
    zero_acc = jnp.zeros((head_count, shard_rows, value_width), jnp.float32)
    start_state = (floor_max, zero_sum, zero_acc, floor_max, zero_sum, zero_acc)
    running = start_state
    key_piece = lax.all_gather(keys, "ep", axis=0, tiled=True)
    value_piece = lax.all_gather(values, "ep", axis=0, tiled=True)
    blocks = key_piece.shape[0] // shard_rows
    key_blocks = key_piece.reshape(blocks, shard_rows, head_count, key_piece.shape[2])
    value_blocks = value_piece.reshape(blocks, shard_rows, head_count, value_width)

    def visit_block(state, inputs):
        key_block, value_block, block_index = inputs
        block_start = block_index * shard_rows
        state = lax.cond(
            block_start <= query_start + shard_rows - 1,
            lambda state_in: update(state_in, key_block, value_block, block_start),
            lambda state_in: state_in,
            state,
        )
        return (state, None)

    running, unused = lax.scan(
        visit_block, running, (key_blocks, value_blocks, lax.iota(jnp.int32, blocks))
    )
    state = running
    diff = state[2] / state[1][:, :, None] - mixing[:, None, None] * state[5] / state[4][:, :, None]
    normed = diff * lax.rsqrt(jnp.mean(diff * diff, axis=2, keepdims=True) + 1e-05) * head_gain
    return normed.astype(jnp.bfloat16)


def mixer_half(queries, keys, values, mixing, head_gain, out_weight):
    attended = attend_heads(queries, keys, values, mixing, head_gain)
    return lax.psum_scatter(
        jnp.einsum("hqe,hed->qd", attended, out_weight, preferred_element_type=jnp.float32).astype(
            jnp.bfloat16
        ),
        "tp",
        scatter_dimension=0,
        tiled=True,
    )


def expert_half(
    tokens_b, norm_gain, expert_ids, group_gate, expert_gate, gate_weight, up_weight, down_weight
):
    local_rows = tokens_b.shape[0]
    width = tokens_b.shape[1]
    top_count = expert_ids.shape[1]
    ep_count = lax.axis_size("ep")
    local_count = gate_weight.shape[0]
    expert_total = ep_count * local_count
    capacity = 3 * local_rows * top_count // (2 * expert_total)
    tokens_f = tokens_b.astype(jnp.float32)
    normed = (
        tokens_f
        * lax.rsqrt(jnp.mean(tokens_f * tokens_f, axis=1, keepdims=True) + 1e-06)
        * norm_gain
    ).astype(jnp.bfloat16)
    flat_ids = expert_ids.reshape(-1)
    one_hot = (flat_ids[:, None] == lax.iota(jnp.int32, expert_total)[None, :]).astype(jnp.int32)
    slot_rank = jnp.sum((jnp.cumsum(one_hot, axis=0) - one_hot) * one_hot, axis=1)
    slot_index = flat_ids * capacity + slot_rank
    owners = jnp.full((expert_total * capacity,), local_rows, jnp.int32)
    owners = owners.at[slot_index].set(lax.iota(jnp.int32, local_rows * top_count) // top_count)
    padded = jnp.concatenate([normed, jnp.zeros((1, width), jnp.bfloat16)], axis=0)
    outgoing = padded[owners].reshape(ep_count, local_count * capacity, width)
    incoming = lax.all_to_all(outgoing, "ep", split_axis=0, concat_axis=0, tiled=True)
    expert_rows = jnp.transpose(
        incoming.reshape(ep_count, local_count, capacity, width), (1, 0, 2, 3)
    )
    expert_rows = expert_rows.reshape(local_count, ep_count * capacity, width)
    piece_gate = lax.all_gather(gate_weight, "tp", axis=2, tiled=True)
    piece_up = lax.all_gather(up_weight, "tp", axis=2, tiled=True)
    piece_down = lax.all_gather(down_weight, "tp", axis=2, tiled=True)
    gate_part = jnp.einsum(
        "jrd,jdf->jrf", expert_rows, piece_gate, preferred_element_type=jnp.float32
    )
    up_part = jnp.einsum("jrd,jdf->jrf", expert_rows, piece_up, preferred_element_type=jnp.float32)
    hidden = (jax.nn.silu(gate_part) * up_part).astype(jnp.bfloat16)
    expert_out = jnp.einsum(
        "jrf,jdf->jrd", hidden, piece_down, preferred_element_type=jnp.float32
    ).astype(jnp.bfloat16)
    outbound = jnp.transpose(
        expert_out.reshape(local_count, ep_count, capacity, width), (1, 0, 2, 3)
    )
    outbound = outbound.reshape(ep_count, local_count * capacity, width)
    returned = lax.all_to_all(outbound, "ep", split_axis=0, concat_axis=0, tiled=True).reshape(
        expert_total * capacity, width
    )
    picked = returned[slot_index].reshape(local_rows, top_count, width).astype(jnp.float32)
    route_weight = group_gate[:, None] * expert_gate
    return jnp.sum(route_weight[:, :, None] * picked, axis=1).astype(jnp.bfloat16)


def per_device(
    queries,
    keys,
    values,
    mixing,
    head_gain,
    out_weight,
    tokens_b,
    norm_gain,
    expert_ids,
    group_gate,
    expert_gate,
    gate_weight,
    up_weight,
    down_weight,
):
    mixed = mixer_half(queries, keys, values, mixing, head_gain, out_weight)
    routed = expert_half(
        tokens_b,
        norm_gain,
        expert_ids,
        group_gate,
        expert_gate,
        gate_weight,
        up_weight,
        down_weight,
    )
    return (mixed, routed)


def solution(mesh):
    placed = (
        P("ep", "tp", None),
        P("ep", "tp", None),
        P("ep", "tp", None),
        P("tp"),
        P(),
        P("tp", None, None),
        P(("ep", "tp"), None),
        P(),
        P(("ep", "tp"), None),
        P(("ep", "tp")),
        P(("ep", "tp"), None),
        P("ep", None, "tp"),
        P("ep", None, "tp"),
        P("ep", None, "tp"),
    )
    return jax.shard_map(
        per_device,
        mesh=mesh,
        in_specs=placed,
        out_specs=(P(("ep", "tp"), None), P(("ep", "tp"), None)),
        check_vma=False,
    )
```

profile of v0, /device:TPU:0, one launch (start us, length us, event | category | flops | bytes accessed | tf_op | source)
XLA Modules:
  0.0 260.2 jit_solution(6079203360803837472)
XLA Ops:
  7.3 1.8 copy.24
  9.1 1.7 copy.25
  10.9 0.7 all-gather.10.cloned.1.call-update
  13.4 1.2 reduce-window.6
  15.3 1.4 scatter_custom_fusion
  17.0 1.0 fusion.33
  17.9 21.8 %all-gather.6.cloned.1.call-done = bf16[2048,2,128]{2,0,1:T(8,128)(2,1)} async-done(((bf16[512,2,128]{2,0,1:T(8,128)(2,1)}), bf16[2048,2,128]{2,0,1:T(8,128)(2,1)}) %all-gather.6.cloned.1.call-update) | async-done | bytes 1048592 | tf_op jit(solution)/shard_map/all_gather | solution.py:54
  39.7 2.3 copy.26
  42.0 26.1 %all-gather.8.cloned.1.call-done = bf16[2048,2,128]{2,0,1:T(8,128)(2,1)} async-done(((bf16[512,2,128]{2,0,1:T(8,128)(2,1)}), bf16[2048,2,128]{2,0,1:T(8,128)(2,1)}) %all-gather.8.cloned.1.call-update) | async-done | bytes 1048592 | tf_op jit(solution)/shard_map/all_gather | solution.py:55
  68.1 1.3 copy.28
  69.5 9.8 %while.23 = (s32[]{:T(128)}, f32[2,512]{1,0:T(2,128)S(1)}, f32[2,512]{1,0:T(2,128)S(1)}, f32[2,512,128]{2,1,0:T(8,128)S(1)}, f32[2,512]{1,0:T(2,128)S(1)}, /*ind...) while((s32[]{:T(128)}, f32[2,512]{1,0:T(2,128)S(1)}, ...), condition=%wide.region_7.8_spmd.clone, body=%wide.region_0.7_spmd.clone.sunk | while | flops 410784768 | bytes 17183128 | solution.py:71
  69.6 0.6 dynamic_slice.36
  70.8 4.6 %conditional.3 = ((f32[2,512]{1,0:T(2,128)S(1)}, f32[2,512]{1,0:T(2,128)S(1)}, f32[2,512,128]{2,1,0:T(8,128)S(1)}, f32[2,512]{1,0:T(2,128)S(1)}, f32[2,512]{1,0:T(2,128)S(1)}, /*index=5*/f32[2,512,128]{2,1,0:T(8,128)S(1)})) conditional(s32[]{:T(128)} %convert_element_type.87, (f32[2,512]{1,0:T(2,128)S(1)}, f32[2,512]{1,0:T(2,128)S(1)}, ...), branch_computations={%region_1.1_spmd, %region_2.6_spmd} | conditional | flops 410784768 | bytes 17180748 | solution.py:63
  70.8 1.0 dynamic-slice_bitcast_fusion
  72.1 0.6 fusion.45
  73.0 0.6 fusion.46
  74.0 0.7 convolution_add_fusion
  74.7 0.7 convolution_add_fusion.1
  75.5 0.6 dynamic_slice.36
  76.8 0.6 dynamic_slice.36
  79.9 2.1 bitcast_convert_fusion
  82.2 2.5 gather_fusion
  84.6 36.1 %all_to_all.10 = bf16[4,96,2048]{2,1,0:T(8,128)(2,1)} all-to-all(bf16[4,96,2048]{2,1,0:T(8,128)(2,1)S(1)} %bitcast.62), channel_id=1, replica_groups=mesh['ep'=4,'tp'=8] {'ep'}, dimensions={0} | all-to-all | bytes 3145728 | tf_op jit(solution)/shard_map/all_to_all | solution.py:116
  120.7 5.7 %fusion.24 = f32[384,1024]{1,0:T(8,128)} fusion(bf16[384,2048]{1,0:T(8,128)(2,1)} %bitcast.63, bf16[1,2048,1024]{2,1,0:T(8,128)(2,1)} %all-gather.10.cloned.1.call-done), kind=kOutput, calls=%fused_computation.38 | convolution fusion | flops 1610612736 | bytes 7340032 | tf_op jit(solution)/shard_map/jrd,jdf->jrf/dot_general | solution.py:124
  126.4 38.6 %all-gather.12.cloned.1.call-done = bf16[1,2048,1024]{2,1,0:T(8,128)(2,1)} async-done(((bf16[1,2048,128]{2,1,0:T(8,128)(2,1)}), bf16[1,2048,1024]{2,1,0:T(8,128)(2,1)}) %all-gather.12.cloned.1.call-update) | async-done | bytes 4194320 | tf_op jit(solution)/shard_map/all_gather | solution.py:122
  165.0 47.5 %all-gather.14.cloned.1.call-done = bf16[1,2048,1024]{2,1,0:T(8,128)(2,1)} async-done(((bf16[1,2048,128]{2,1,0:T(8,128)(2,1)}), bf16[1,2048,1024]{2,1,0:T(8,128)(2,1)}) %all-gather.14.cloned.1.call-update) | async-done | bytes 4194320 | tf_op jit(solution)/shard_map/all_gather | solution.py:123
  212.5 8.6 %fusion.26 = bf16[384,2048]{1,0:T(8,128)(2,1)} fusion(bf16[1,2048,1024]{2,1,0:T(8,128)(2,1)} %all-gather.14.cloned.1.call-done, f32[384,1024]{1,0:T(8,128)} %fusion.24, bf16[384,2048]{1,0:T(8,128)(2,1)S(1)} %bitcast.64, bf16[1,2048,1024]{2,1,0:T(8,128)(2,1)} %all-gather.12.cloned.1.call-done), kind=kOutput, calls=%fused_computation.41 | convolution fusion | flops 3224371200 | bytes 13107200 | tf_op jit(solution)/shard_map/jrf,jdf->jrd/dot_general | solution.py:129
  221.1 3.8 %all-to-all-start.1 = ((bf16[4,96,2048]{2,1,0:T(8,128)(2,1)}), bf16[4,96,2048]{2,1,0:T(8,128)(2,1)S(1)}, u32[]{:S(2)}, u32[]{:S(2)}) async-start(bf16[4,96,2048]{2,1,0:T(8,128)(2,1)} %bitcast.65), calls=%async_computation.2 | async-start | bytes 3145728 | tf_op jit(solution)/shard_map/all_to_all | solution.py:136
  225.0 19.7 %all-to-all-done.1 = bf16[4,96,2048]{2,1,0:T(8,128)(2,1)S(1)} async-done(((bf16[4,96,2048]{2,1,0:T(8,128)(2,1)}), bf16[4,96,2048]{2,1,0:T(8,128)(2,1)S(1)}, u32[]{:S(2)}, u32[]{:S(2)}) %all-to-all-start.1) | async-done | bytes 1572896 | tf_op jit(solution)/shard_map/all_to_all | solution.py:136
  244.7 2.3 gather_fusion.1
  247.1 2.4 reshape.163
  249.4 3.9 %multiply_reduce_fusion = bf16[128,2048]{1,0:T(8,128)(2,1)} fusion(f32[128,2,2048]{2,1,0:T(2,128)S(1)} %reshape.163, f32[128,2]{1,0:T(8,128)S(1)} %copy.29), kind=kLoop, calls=%fused_computation.42 | loop fusion | flops 786432 | bytes 2622464 | tf_op jit(solution)/shard_map/reduce_sum | solution.py:141
  (87 shorter events, 5.1 us)
Async XLA Ops:
  7.2 72.7 %copy-start = (bf16[2,128,2048]{2,1,0:T(8,128)(2,1)S(1)}, bf16[2,128,2048]{2,1,0:T(8,128)(2,1)}, u32[]{:S(2)}) copy-start(bf16[2,128,2048]{2,1,0:T(8,128)(2,1)} %param.23) | copy-start | bytes 3145732
  7.2 5.6 %copy-start.6 = (s32[128,2]{0,1:T(2,128)S(1)}, s32[128,2]{0,1:T(2,128)}, u32[]{:S(2)}) copy-start(s32[128,2]{0,1:T(2,128)} %param.26) | copy-start | bytes 3076
  7.2 6.0 %copy-start.4 = (bf16[512,2,128]{2,1,0:T(2,128)(2,1)S(1)}, bf16[512,2,128]{2,1,0:T(2,128)(2,1)}, u32[]{:S(2)}) copy-start(bf16[512,2,128]{2,1,0:T(2,128)(2,1)} %param.18) | copy-start | bytes 786436
  7.2 9.5 %copy-start.1 = (bf16[128,2048]{1,0:T(8,128)(2,1)S(1)}, bf16[128,2048]{1,0:T(8,128)(2,1)}, u32[]{:S(2)}) copy-start(bf16[128,2048]{1,0:T(8,128)(2,1)} %param.24) | copy-start | bytes 1572868
  7.2 32.5 %all-gather.6.cloned.1.call-start = ((), (), s32[]{:S(2)}) async-start(), calls=%async_computation.3 | async-start | bytes 1310720 | tf_op jit(solution)/shard_map/all_gather | solution.py:54
  9.1 7.9 %copy-start.5 = (f32[2048]{0:T(1024)S(1)}, f32[2048]{0:T(1024)}, u32[]{:S(2)}) copy-start(f32[2048]{0:T(1024)} %param.25) | copy-start | bytes 24580
  9.1 59.0 %all-gather.8.cloned.1.call-start = ((), (), s32[]{:S(2)}) async-start(), calls=%async_computation.4 | async-start | bytes 1310720 | tf_op jit(solution)/shard_map/all_gather | solution.py:55
  10.8 109.8 %all-gather.10.cloned.1.call-start = ((), (), s32[]{:S(2)}) async-start(), calls=%async_computation.6 | async-start | bytes 4718592 | tf_op jit(solution)/shard_map/all_gather | solution.py:121
  11.6 153.4 %all-gather.12.cloned.1.call-start = ((), (), s32[]{:S(2)}) async-start(), calls=%async_computation.7 | async-start | bytes 4718592 | tf_op jit(solution)/shard_map/all_gather | solution.py:122
  12.2 200.3 %all-gather.14.cloned.1.call-start = ((), (), s32[]{:S(2)}) async-start(), calls=%async_computation.8 | async-start | bytes 4718592 | tf_op jit(solution)/shard_map/all_gather | solution.py:123
  12.7 240.6 %reduce-scatter.2.cloned.1.call-start = ((), (), s32[]{:S(2)}) async-start(), calls=%async_computation.5 | async-start | bytes 2359296 | tf_op jit(solution)/shard_map/reduce_scatter | solution.py:82
  69.5 9.9 %copy-start.8 = (f32[2]{0:T(128)S(1)}, f32[2]{0:T(128)}, u32[]{:S(2)}) copy-start(f32[2]{0:T(128)} %param.21) | copy-start | bytes 28
  69.5 10.4 %copy-start.9 = (f32[128]{0:T(128)S(1)}, f32[128]{0:T(128)}, u32[]{:S(2)}) copy-start(f32[128]{0:T(128)} %param.22) | copy-start | bytes 1540
  79.9 2.2 copy-start.2
  120.7 91.8 %copy-start.3 = (bf16[4,96,2048]{2,1,0:T(8,128)(2,1)S(1)}, bf16[4,96,2048]{2,1,0:T(8,128)(2,1)}, u32[]{:S(2)}) copy-start(bf16[4,96,2048]{2,1,0:T(8,128)(2,1)} %all_to_all.10) | copy-start | bytes 4718596
  221.1 3.8 %copy-start.7 = (f32[128,2]{0,1:T(2,128)S(1)}, f32[128,2]{0,1:T(2,128)}, u32[]{:S(2)}) copy-start(f32[128,2]{0,1:T(2,128)} %param.28) | copy-start | bytes 3076
  221.1 3.8 %copy-start.10 = (f32[128]{0:T(128)S(1)}, f32[128]{0:T(128)}, u32[]{:S(2)}) copy-start(f32[128]{0:T(128)} %param.27) | copy-start | bytes 1540
  221.1 23.6 %all-to-all-start.1 = ((bf16[4,96,2048]{2,1,0:T(8,128)(2,1)}), bf16[4,96,2048]{2,1,0:T(8,128)(2,1)S(1)}, u32[]{:S(2)}, u32[]{:S(2)}) async-start(bf16[4,96,2048]{2,1,0:T(8,128)(2,1)} %bitcast.65), calls=%async_computation.2 | async-start | bytes 3145728 | tf_op jit(solution)/shard_map/all_to_all | solution.py:136
Sparse Core Ops, SparseCore 0:
  10.4 29.2 all-gather.5
  41.5 26.4 all-gather.7
  69.7 47.8 all-gather.9
  119.0 45.9 all-gather.11
  166.4 45.9 all-gather.13
  215.2 34.1 reduce-scatter.1
where the time goes:
time: 261 us; the launch traced here: 260 us
  waiting for transfers between devices  155 us (59%)
  blocking collectives  36.1 us (14%)
  local copies, waits for them, and re-layouts  20.4 us (8%)
  matrix products  19.2 us (7%)
  between operations  14.4 us (6%)
  other arithmetic  7.89 us (3%)
  starting transfers between devices  4.02 us (2%)
  loops' own time  2.93 us (1%)
    all_gather x1, waiting for transfers between devices, expert_half(): piece_down = lax.all_gather(down_weight, 'tp', axis=2, tiled=True)  47.5 us
    all_gather x1, waiting for transfers between devices, expert_half(): piece_up = lax.all_gather(up_weight, 'tp', axis=2, tiled=True)  38.6 us
    all_to_all x1, blocking collectives, expert_half(): lax.all_to_all(outgoing, 'ep', split_axis=0, concat_axis=0, tiled=True)  36.1 us
    all_gather x1, waiting for transfers between devices, attend_heads(): value_piece = lax.all_gather(values, 'ep', axis=0, tiled=True)  26.1 us
    all_gather x1, waiting for transfers between devices, attend_heads(): key_piece = lax.all_gather(keys, 'ep', axis=0, tiled=True)  21.8 us
    all_to_all x1, waiting for transfers between devices, expert_half(): lax.all_to_all(outbound, 'ep', split_axis=0, concat_axis=0, tiled=True)  19.7 us
    dot_general x1, matrix products, expert_half(): jnp.einsum('jrf,jdf->jrd', hidden, piece_down, preferred_element_type=jnp...  8.63 us
    unnamed x28, local copies, waits for them, and re-layouts  7.42 us
  transfers between devices with their start and end apart: 7, of which 5 were waited for; matrix products, arithmetic and copies ran while one was open for 18% of the time, Pallas kernels for 0%

commit v1 on v0

v1 whole, which is shorter than its diff:
```python
import functools
import math

import jax
import jax.numpy as jnp
from jax import lax
from jax.experimental import pallas as pl
from jax.experimental.pallas import tpu as pltpu
from jax.sharding import PartitionSpec as P

HEAD = 64
CHUNKS = 4
F32 = jnp.float32
BF16 = jnp.bfloat16
MESH = pl.DeviceIdType.MESH
NT = (((1,), (1,)), ((), ()))


def kernel(
    ep,
    tp,
    mix_ref,
    q_ref,
    kv_ref,
    gain_ref,
    ow_ref,
    tok_ref,
    norm_ref,
    ids_ref,
    group_ref,
    gates_ref,
    gate_ref,
    up_ref,
    dn_ref,
    mixed_ref,
    routed_ref,
    kv_all,
    w_gu,
    w_dn,
    rows_x,
    acc,
    hid,
    give,
    take,
    back,
    ret,
    att,
    part,
    pair,
    chip_sum,
    landed,
    line_out,
    out_ref,
    place_ref,
    route_ref,
    local_sem,
    kv_s,
    kv_r,
    x_s,
    x_r,
    xp_s,
    xp_r,
    gu_s,
    gu_r,
    dn_s,
    dn_r,
    pr_s,
    pr_r,
    rs_s,
    rs_r,
    o_s,
    o_r,
    b_s,
    b_r,
):
    chips = tp // 2
    me = lax.axis_index("ep")
    mine = lax.axis_index("tp")
    z = mine // 2
    core = mine % 2
    other = z * 2 + 1 - core
    heads, length, wide = q_ref.shape
    cap = out_ref.shape[1]
    half = ep * cap
    unit = dn_ref.shape[2]
    step = dn_ref.shape[1]
    joined = gate_ref.shape[1] != unit

    def remote(src, dst, send, recv, target):
        return pltpu.make_async_remote_copy(
            src_ref=src,
            dst_ref=dst,
            send_sem=send,
            recv_sem=recv,
            device_id=target,
            device_id_type=MESH,
        )

    barrier = pltpu.get_barrier_semaphore()
    for s in range(1, ep):
        pl.semaphore_signal(
            barrier, inc=1, device_id={"ep": (me + s) % ep}, device_id_type=MESH
        )
    for s in range(1, tp):
        pl.semaphore_signal(
            barrier, inc=1, device_id={"tp": (mine + s) % tp}, device_id_type=MESH
        )
    pl.semaphore_wait(barrier, ep + tp - 2)

    def gu_copy(src, side):
        target = (z + 1 - 2 * side) * 2 + core
        return remote(
            w_gu.at[src], w_gu.at[src], gu_s.at[side, src], gu_r.at[src], {"tp": target}
        )

    def dn_copy(src, c, side):
        target = (z + 1 - 2 * side) * 2 + core
        return remote(
            w_dn.at[src, c],
            w_dn.at[src, c],
            dn_s.at[side, src, c],
            dn_r.at[src, c],
            {"tp": target},
        )

    def has_next(side):
        return (z < chips - 1) if side == 0 else (z > 0)

    def source(k, side):
        return z - k if side == 0 else z + k

    def exists(k, side):
        return (z >= k) if side == 0 else (z + k <= chips - 1)

    own = [
        pltpu.make_async_copy(
            gate_ref, w_gu.at[z] if joined else w_gu.at[z, :, pl.ds(0, unit)], local_sem.at[0]
        ),
        pltpu.make_async_copy(dn_ref, w_dn.at[z], local_sem.at[1]),
        pltpu.make_async_copy(kv_ref, kv_all.at[0], local_sem.at[2]),
        pltpu.make_async_copy(out_ref.at[0], rows_x.at[pl.ds(0, cap)], local_sem.at[3]),
    ]
    if not joined:
        own.append(
            pltpu.make_async_copy(up_ref, w_gu.at[z, :, pl.ds(unit, unit)], local_sem.at[4])
        )
    for copy in own[:3] + own[4:]:
        copy.start()

    def kv_copy(s):
        return remote(kv_ref, kv_all.at[s], kv_s.at[s], kv_r.at[s], {"ep": lax.rem(me + s, ep)})

    for s in range(1, ep):
        pl.when(me + s < ep)(lambda s=s: kv_copy(s).start())
    own[0].wait()
    if not joined:
        own[4].wait()
    for side in range(2):
        pl.when(has_next(side))(lambda side=side: gu_copy(z, side).start())
    own[1].wait()
    for side in range(2):

        @pl.when(has_next(side))
        def _(side=side):
            for c in range(CHUNKS):
                dn_copy(z, c, side).start()

    def x_copy(s):
        return remote(
            out_ref.at[s],
            rows_x.at[pl.ds(s * cap, cap)],
            x_s.at[s],
            x_r.at[s],
            {"ep": lax.rem(me + s, ep)},
        )

    def xp_copy(s):
        src = rows_x.at[pl.ds(s * cap, cap)]
        dst = rows_x.at[pl.ds(half + s * cap, cap)]
        return remote(src, dst, xp_s.at[s], xp_r.at[s], {"tp": other})

    def pass_gu(k):
        for side in range(2):

            @pl.when(exists(k, side) & has_next(side))
            def _(side=side):
                src = source(k, side)
                gu_copy(src, side).wait_recv()
                gu_copy(src, side).start()

    def pass_dn(k, c):
        for side in range(2):

            @pl.when(exists(k, side) & has_next(side))
            def _(side=side):
                src = source(k, side)
                dn_copy(src, c, side).wait_recv()
                dn_copy(src, c, side).start()

    tokens = tok_ref[...].astype(F32)
    normed = (
        tokens
        * lax.rsqrt(jnp.mean(tokens * tokens, axis=1, keepdims=True) + 1e-06)
        * norm_ref[...]
    ).astype(BF16)
    local_rows = tok_ref.shape[0]
    relative = ids_ref[...] - me
    relative = jnp.where(relative < 0, relative + ep, relative)
    expert_lane = lax.broadcasted_iota(jnp.int32, (local_rows, ep), 1)
    named = jnp.zeros((local_rows, ep), F32)
    route = jnp.zeros((local_rows, ep), F32)
    for k in range(ids_ref.shape[1]):
        hit = expert_lane == relative[:, k : k + 1]
        named = jnp.where(hit, 1.0, named)
        route = route + jnp.where(hit, group_ref[...] * gates_ref[:, k : k + 1], 0.0)
    route_ref[...] = route
    square = (local_rows, local_rows)
    before = jnp.where(
        lax.broadcasted_iota(jnp.int32, square, 1) < lax.broadcasted_iota(jnp.int32, square, 0),
        1.0,
        0.0,
    ).astype(BF16)
    rank = jnp.dot(before, named.astype(BF16), preferred_element_type=F32)
    rank = jnp.where(named > 0.5, rank, -1.0).astype(jnp.int32)
    slot_lane = lax.broadcasted_iota(jnp.int32, (local_rows, cap), 1)
    for s in list(range(1, ep)) + [0]:
        place = jnp.where(rank[:, s : s + 1] == slot_lane, 1.0, 0.0).astype(BF16)
        place_ref[s] = place
        out_ref[s] = lax.dot_general(
            place, normed, (((0,), (0,)), ((), ())), preferred_element_type=F32
        ).astype(BF16)
        if s:
            x_copy(s).start()
    own[3].start()
    own[3].wait()
    xp_copy(0).start()

    own[2].wait()
    for s in range(1, ep):
        pl.when(me >= s)(lambda s=s: kv_copy(s).wait_recv())
    if chips > 2:
        pass_gu(1)
    tile = min(256, length)
    tiles = length // tile

    def attend(index, carry):
        h = index // tiles
        start = pl.multiple_of((index % tiles) * tile, tile)
        q = q_ref[h, pl.ds(start, tile), :]
        lane = lax.broadcasted_iota(jnp.int32, (tile, wide), 1)
        ratio = []
        for m in range(2):
            pick = (lane < HEAD) if m == 0 else (lane >= HEAD)
            q_map = jnp.where(pick, q, jnp.zeros_like(q))

            def visit(s, state, diagonal=False, q_map=q_map):
                top, total, value = state
                scores = lax.dot_general(
                    q_map, kv_all[s, h, :, :wide], NT, preferred_element_type=F32
                )
                if diagonal:
                    row = start + lax.broadcasted_iota(jnp.int32, scores.shape, 0)
                    col = lax.broadcasted_iota(jnp.int32, scores.shape, 1)
                    scores = jnp.where(col <= row, scores, -1e30)
                fresh = jnp.maximum(top, jnp.max(scores, axis=1, keepdims=True))
                shrink = jnp.exp(top - fresh)
                expo = jnp.exp(scores - fresh)
                total = total * shrink + jnp.sum(expo, axis=1, keepdims=True)
                value = value * shrink + jnp.dot(
                    expo.astype(BF16), kv_all[s, h, :, wide:], preferred_element_type=F32
                )
                return fresh, total, value

            state = (
                jnp.full((tile, 1), -1e30, F32),
                jnp.zeros((tile, 1), F32),
                jnp.zeros((tile, kv_ref.shape[2] - wide), F32),
            )
            state = visit(0, state, True)
            state = lax.fori_loop(1, me + 1, visit, state)
            ratio.append(state[2] / state[1])
        diff = ratio[0] - mix_ref[h] * ratio[1]
        scaled = diff * lax.rsqrt(jnp.mean(diff * diff, axis=1, keepdims=True) + 1e-05)
        att[h, pl.ds(start, tile), :] = (scaled * gain_ref[...]).astype(BF16)
        return carry

    lax.fori_loop(0, heads * tiles, attend, 0)

    block = length // tp

    def project(t, carry):
        rows = pl.ds(pl.multiple_of(t * 2 * block, 2 * block), 2 * block)
        total = 0.0
        for h in range(heads):
            total = total + jnp.dot(att[h, rows, :], ow_ref[h], preferred_element_type=F32)
        part[0, t] = total[:block].astype(BF16)
        part[1, t] = total[block:].astype(BF16)
        return carry

    lax.fori_loop(0, chips, project, 0)
    pair_copy = remote(part.at[1 - core], pair, pr_s, pr_r, {"tp": other})
    pair_copy.start()
    for s in range(1, ep):
        x_copy(s).wait_recv()
        xp_copy(s).start()
    pair_copy.wait_recv()

    def add_pair(t, carry):
        chip_sum[t] = (part[core, t].astype(F32) + pair[t].astype(F32)).astype(BF16)
        return carry

    lax.fori_loop(0, chips, add_pair, 0)

    def line_copy(side, t, first):
        return remote(
            chip_sum.at[t] if first else line_out.at[side, t],
            landed.at[side, t],
            rs_s.at[side, t],
            rs_r.at[side, t],
            {"tp": (z + 1 - 2 * side) * 2 + core},
        )

    def stage_each(k, do):
        for side in range(2):
            at = k if side == 0 else chips - 1 - k
            targets = range(chips - 1, k, -1) if side == 0 else range(chips - 1 - k)

            @pl.when(z == at)
            def _(side=side, targets=targets):
                for t in targets:
                    do(side, t, k == 0)

    def stage_send(side, t, first):
        copy = line_copy(side, t, first)
        if not first:
            copy.wait_recv()
            line_out[side, t] = (
                chip_sum[t].astype(F32) + landed[side, t].astype(F32)
            ).astype(BF16)
        copy.start()

    stage_each(0, stage_send)

    m_tile = 256 if (2 * half) % 256 == 0 else cap
    m_count = 2 * half // m_tile

    def hidden_of(src):
        def one(t, carry):
            rows = pl.ds(pl.multiple_of(t * m_tile, m_tile), m_tile)
            product = jnp.dot(rows_x[rows, :], w_gu[src], preferred_element_type=F32)
            gate = product[:, :unit]
            hid[src, rows, :] = (
                gate / (1.0 + jnp.exp(-gate)) * product[:, unit:]
            ).astype(BF16)
            return carry

        lax.fori_loop(0, m_count, one, 0)

    def down_of(src, c, first=False):
        def one(t, carry):
            rows = pl.ds(pl.multiple_of(t * m_tile, m_tile), m_tile)
            product = lax.dot_general(
                hid[src, rows, :], w_dn[src, c], NT, preferred_element_type=F32
            )
            if first:
                acc[c, rows, :] = product
            else:
                acc[c, rows, :] += product
            return carry

        lax.fori_loop(0, m_count, one, 0)

    def use_gu(k):
        for side in range(2):

            @pl.when(exists(k, side))
            def _(side=side):
                src = source(k, side)
                pl.when(jnp.logical_not(has_next(side)))(lambda: gu_copy(src, side).wait_recv())
                hidden_of(src)

    def use_dn(k, c):
        for side in range(2):

            @pl.when(exists(k, side))
            def _(side=side):
                src = source(k, side)
                pl.when(jnp.logical_not(has_next(side)))(
                    lambda: dn_copy(src, c, side).wait_recv()
                )
                down_of(src, c)

    last = chips - 1
    late = [k for k in (last - 2, last - 1) if k >= 1]
    for s in range(ep):
        xp_copy(s).wait_recv()
    hidden_of(z)
    for c in range(CHUNKS):
        down_of(z, c, True)
    for k in range(1, last):
        if k + 1 < last:
            pass_gu(k + 1)
        use_gu(k)
        if k < last - 2:
            for c in range(CHUNKS):
                pass_dn(k, c)
        elif k == late[0]:
            for c in range(CHUNKS):
                for near in late:
                    pass_dn(near, c)
        stage_each(k, stage_send)
        if k < last - 1:
            for c in range(CHUNKS):
                use_dn(k, c)
    if last > 0:
        use_gu(last)

    def give_copy(c):
        return remote(give.at[c], take.at[c], o_s.at[c], o_r.at[c], {"tp": other})

    def back_copy(c, s):
        return remote(
            back.at[c, s],
            ret.at[c, s],
            b_s.at[c, s],
            b_r.at[c, s],
            {"ep": lax.rem(me + ep - s, ep)},
        )

    def combine(c):
        total = 0.0
        for s in range(ep):
            if s == 0:
                block_rows = back[c, 0]
            else:
                back_copy(c, s).wait_recv()
                block_rows = ret[c, s]
            picked = jnp.dot(place_ref[s], block_rows, preferred_element_type=F32)
            total = total + route_ref[:, s : s + 1] * picked
        routed_ref[:, c * step : (c + 1) * step] = total.astype(BF16)

    for c in range(CHUNKS):
        for k in range(max(last - 1, 1), last + 1):
            use_dn(k, c)
        give[c] = acc[c, half:, :].astype(BF16)
        give_copy(c).start()
        give_copy(c).wait_recv()
        for s in range(ep):
            rows = slice(s * cap, (s + 1) * cap)
            back[c, s] = (acc[c, rows, :] + take[c, rows, :].astype(F32)).astype(BF16)
        for s in range(1, ep):
            back_copy(c, s).start()
        if c > 1:
            combine(c - 2)
    mixed_ref[...] = chip_sum[z]
    for side in range(2):

        @pl.when((z > 0) if side == 0 else (z < chips - 1))
        def _(side=side):
            line_copy(side, z, False).wait_recv()
            mixed_ref[...] = (
                mixed_ref[...].astype(F32) + landed[side, z].astype(F32)
            ).astype(BF16)

    for c in range(max(CHUNKS - 2, 0), CHUNKS):
        combine(c)

    for s in range(1, ep):
        pl.when(me + s < ep)(lambda s=s: kv_copy(s).wait_send())
        x_copy(s).wait_send()
    for s in range(ep):
        xp_copy(s).wait_send()
    for k in range(chips - 1):
        for side in range(2):

            @pl.when(exists(k, side) & has_next(side))
            def _(side=side, k=k):
                src = source(k, side)
                gu_copy(src, side).wait_send()
                for c in range(CHUNKS):
                    dn_copy(src, c, side).wait_send()

    pair_copy.wait_send()
    for k in range(chips - 1):
        stage_each(k, lambda side, t, first: line_copy(side, t, first).wait_send())
    for c in range(CHUNKS):
        give_copy(c).wait_send()
        for s in range(1, ep):
            back_copy(c, s).wait_send()


def per_device(
    queries,
    keys,
    values,
    mixing,
    head_gain,
    out_weight,
    tokens_b,
    norm_gain,
    expert_ids,
    group_gate,
    expert_gate,
    gate_weight,
    up_weight,
    down_weight,
):
    ep = lax.axis_size("ep")
    tp = lax.axis_size("tp")
    chips = tp // 2
    length, heads, wide = queries.shape
    val = values.shape[2]
    local_rows, width = tokens_b.shape
    top_count = expert_ids.shape[1]
    unit = gate_weight.shape[2]
    assert gate_weight.shape[0] == 1 and wide == 2 * HEAD
    capacity = 3 * local_rows * top_count // (2 * ep)
    cap = -(-capacity // 16) * 16
    step = width // CHUNKS

    scaled = (queries.astype(F32) * (1.0 / math.sqrt(HEAD))).astype(BF16).transpose(1, 0, 2)
    kv = jnp.concatenate([keys, values], axis=2).transpose(1, 0, 2)
    gate, up = gate_weight[0], up_weight[0]
    if unit % 128:
        gate = jnp.concatenate([gate, up], axis=1)
    half = ep * cap
    block = length // tp
    vmem = pl.BlockSpec(memory_space=pltpu.VMEM)
    dma = pltpu.SemaphoreType.DMA
    return pl.pallas_call(
        functools.partial(kernel, ep, tp),
        out_shape=(
            jax.ShapeDtypeStruct((block, width), BF16),
            jax.ShapeDtypeStruct((local_rows, width), BF16),
        ),
        in_specs=[pl.BlockSpec(memory_space=pltpu.SMEM)] + [vmem] * 12,
        out_specs=(vmem, vmem),
        scratch_shapes=[
            pltpu.VMEM((ep, heads, length, wide + val), BF16),
            pltpu.VMEM((chips, width, 2 * unit), BF16),
            pltpu.VMEM((chips, CHUNKS, step, unit), BF16),
            pltpu.VMEM((2 * half, width), BF16),
            pltpu.VMEM((CHUNKS, 2 * half, step), F32),
            pltpu.VMEM((chips, 2 * half, unit), BF16),
            pltpu.VMEM((CHUNKS, half, step), BF16),
            pltpu.VMEM((CHUNKS, half, step), BF16),
            pltpu.VMEM((CHUNKS, ep, cap, step), BF16),
            pltpu.VMEM((CHUNKS, ep, cap, step), BF16),
            pltpu.VMEM((heads, length, val), BF16),
            pltpu.VMEM((2, chips, block, width), BF16),
            pltpu.VMEM((chips, block, width), BF16),
            pltpu.VMEM((chips, block, width), BF16),
            pltpu.VMEM((2, chips, block, width), BF16),
            pltpu.VMEM((2, chips, block, width), BF16),
            pltpu.VMEM((ep, cap, width), BF16),
            pltpu.VMEM((ep, local_rows, cap), BF16),
            pltpu.VMEM((local_rows, ep), F32),
            dma((5,)),
            dma((ep,)),
            dma((ep,)),
            dma((ep,)),
            dma((ep,)),
            dma((ep,)),
            dma((ep,)),
            dma((2, chips)),
            dma((chips,)),
            dma((2, chips, CHUNKS)),
            dma((chips, CHUNKS)),
            dma,
            dma,
            dma((2, chips)),
            dma((2, chips)),
            dma((CHUNKS,)),
            dma((CHUNKS,)),
            dma((CHUNKS, ep)),
            dma((CHUNKS, ep)),
        ],
        compiler_params=pltpu.CompilerParams(
            collective_id=0, has_side_effects=True, vmem_limit_bytes=62 * 1024 * 1024
        ),
    )(
        mixing,
        scaled,
        kv,
        head_gain[None],
        out_weight,
        tokens_b,
        norm_gain[None],
        expert_ids,
        group_gate[:, None],
        expert_gate,
        gate,
        up,
        down_weight[0].reshape(CHUNKS, step, unit),
    )


def solution(mesh):
    placed = (
        P("ep", "tp", None),
        P("ep", "tp", None),
        P("ep", "tp", None),
        P("tp"),
        P(),
        P("tp", None, None),
        P(("ep", "tp"), None),
        P(),
        P(("ep", "tp"), None),
        P(("ep", "tp")),
        P(("ep", "tp"), None),
        P("ep", None, "tp"),
        P("ep", None, "tp"),
        P("ep", None, "tp"),
    )
    return jax.shard_map(
        per_device,
        mesh=mesh,
        in_specs=placed,
        out_specs=(P(("ep", "tp"), None), P(("ep", "tp"), None)),
        check_vma=False,
    )
```

time: 261 us -> 133 us (0.51)
  waiting for transfers between devices: 155 us -> 0 us
  Pallas kernels: 0 us -> 123 us
  blocking collectives: 36.1 us -> 0 us
  matrix products: 19.2 us -> 0 us
  local copies, waits for them, and re-layouts: 20.4 us -> 6.4 us
  between operations: 14.4 us -> 0.67 us
  other arithmetic: 7.89 us -> 2.6 us
  starting transfers between devices: 4.02 us -> 0 us
  loops' own time: 2.93 us -> 0 us
    all_gather x5 -> x0, waiting for transfers between devices: 134 us -> none  [the longest x1 47.5 us: expert_half(): piece_down = lax.all_gather(down_weight, 'tp', axis=2, tiled=True)]
    pallas_call x0 -> x1, Pallas kernels: none -> 123 us  [per_device(): pl.pallas_call(functools.partial(kernel, ep, tp), out_shape=(jax.ShapeDty...]
    all_to_all x1 -> x0, blocking collectives: 36.1 us -> none  [expert_half(): lax.all_to_all(outgoing, 'ep', split_axis=0, concat_axis=0, tiled=True)]
    all_to_all x1 -> x0, waiting for transfers between devices: 19.7 us -> none  [expert_half(): lax.all_to_all(outbound, 'ep', split_axis=0, concat_axis=0, tiled=True)]
    dot_general x7 -> x0, matrix products: 19.2 us -> none  [the longest x1 8.63 us: expert_half(): jnp.einsum('jrf,jdf->jrd', hidden, piece_down, preferred_element_type=jnp...]
    reduce_sum x6 -> x0, other arithmetic: 5.26 us -> none  [the longest x1 3.93 us: expert_half(): jnp.sum(route_weight[:, :, None] * picked, axis=1).astype(jnp.bfloat16)]
    gather x2 -> x0, local copies, waits for them, and re-layouts: 4.78 us -> none  [the longest x1 2.45 us: expert_half(): outgoing = padded[owners].reshape(ep_count, local_count * capacity, width)]
    all_to_all x1 -> x0, starting transfers between devices: 3.79 us -> none  [expert_half(): lax.all_to_all(outbound, 'ep', split_axis=0, concat_axis=0, tiled=True)]
  transfers between devices with their start and end apart: 7 -> 0, of which waited for: 5 -> 0; matrix products, arithmetic and copies ran while one was open for 18% -> 0% of each run, Pallas kernels for 0% -> 0%
where the time goes in v1:
time: 133 us
  Pallas kernels  123 us (92%)
  local copies, waits for them, and re-layouts  6.4 us (5%)
  other arithmetic  2.6 us (2%)
    pallas_call x1, Pallas kernels, per_device(): pl.pallas_call(functools.partial(kernel, ep, tp), out_shape=(jax.ShapeDty...  123 us
    unnamed x18, local copies, waits for them, and re-layouts  5.65 us

profile of v1, /device:TPU:0, one launch (start us, length us, event | category | flops | bytes accessed | tf_op | source)
XLA Modules:
  0.0 132.5 jit_solution(4799795827914490443)
XLA Ops:
  0.6 0.0 copy-start.3
  0.6 0.7 copy-done.3
  1.3 0.0 copy-start.5
  1.3 0.7 copy.19.ids_ref
  2.0 0.0 copy-done.5
  2.0 0.0 copy-start.4
  2.0 0.7 copy.20.group_ref
  2.8 0.0 copy-done.4
  2.8 0.7 copy.21.gates_ref
  3.5 0.0 copy-start.1
  3.5 1.7 %fusion.q_ref = bf16[2,512,128]{2,1,0:T(8,128)(2,1)} fusion(bf16[512,2,128]{2,1,0:T(2,128)(2,1)} %param.14), kind=kLoop, calls=%fused_computation.2 | loop fusion | flops 393216 | bytes 524288 | tf_op jit(solution)/shard_map/transpose | solution.py:521
  5.3 0.0 copy-done.1
  5.3 0.0 copy-start.2
  5.3 0.9 copy-done.2
  6.3 0.9 maximum_bitcast_fusion.kv_ref
  7.1 122.9 %shard_map.149 = (bf16[64,2048]{1,0:T(8,128)(2,1)}, bf16[128,2048]{1,0:T(8,128)(2,1)}) custom-call(f32[2]{0:T(128)} %mix_ref.1, bf16[2,512,128]{2,1,0:T(8,128)(2,1)} %fusion.q_ref, bf16[2,512,256]{2,1,0:T(8,128)(2,1)} %maximum_bitcast_fusion.kv_ref, f32[1,128]{1,0:T(1,128)} %bitcast.15, bf16[2,128,2048]{2,1,0:T(8,128)(2,1)} %ow_ref.1, ...), custom_call_target="tpu_custom_call" | custom-call | tf_op jit(solution)/shard_map/pallas_call | solution.py:530
  130.0 0.0 copy-start
  130.0 1.7 %copy.25 = bf16[64,2048]{1,0:T(8,128)(2,1)} copy(bf16[64,2048]{1,0:T(8,128)(2,1)} %get-tuple-element.4) | data formatting | bytes 524288
  131.7 0.0 copy-done
  131.7 0.8 copy.26
  (2 shorter events, 0.1 us)
Async XLA Ops:
  0.6 0.7 copy-start.3
  1.3 0.7 copy-start.5
  2.0 0.7 copy-start.4
  3.5 1.8 %copy-start.1 = (bf16[512,2,128]{2,1,0:T(2,128)(2,1)S(1)}, bf16[512,2,128]{2,1,0:T(2,128)(2,1)}, u32[]{:S(2)}) copy-start(bf16[512,2,128]{2,1,0:T(2,128)(2,1)} %param.15) | copy-start | bytes 786436
  5.3 1.0 copy-start.2
  130.0 1.7 %copy-start = (bf16[128,2048]{1,0:T(8,128)(2,1)S(1)}, bf16[128,2048]{1,0:T(8,128)(2,1)}, u32[]{:S(2)}) copy-start(bf16[128,2048]{1,0:T(8,128)(2,1)} %get-tuple-element.5) | copy-start | bytes 1572868
